TPU v7x, 32 devices: a whole 2x2x4 slice. The times are simulated.
32 devices in a mesh: rep: 2 (over x), fs: 4 (over z), tp: 4 (over y, core).
Axes of the slice: x: 2, y: 2, z: 4, core: 2. Of those that a mesh axis runs over, the one named last changes fastest.
Arguments:
- tokens: bfloat16 [4096, 2048], P(('rep', 'fs', 'tp')), may hold values from -6 to 6
- norm_gain: float32 [2048], replicated, may hold values from 0.1 to 1.9
- gate_weight: float32 [2048, 5632], P('fs', 'tp'), may hold values from -0.125 to 0.125
- gate_scale: float32 [5632], P('tp'), may hold values from 0.5 to 2
- up_weight: float32 [2048, 5632], P('fs', 'tp'), may hold values from -0.125 to 0.125
- up_scale: float32 [5632], P('tp'), may hold values from 0.5 to 2
- down_weight: float32 [5632, 2048], P('tp', 'fs'), may hold values from -0.078125 to 0.078125
- down_scale: float32 [2048], P('fs'), may hold values from 0.5 to 2
Outputs:
- mixed: bfloat16 [4096, 2048], P(('rep', 'fs', 'tp'))
All inputs are finite; a program needn't handle non-finite values.
Results may differ from a plain program's by a relative error of at most 0.014.
Values may be sent and summed in bfloat16 or wider, within the bound.
No kernel may reach another device: no remote copies, remote signals or barrier semaphores. Data moves between devices by JAX's collectives and lax.ppermute only.
A program may use at most 64 MiB of HBM per device.

v0:
```python
import jax
import jax.numpy as jnp
from jax import lax
from jax.sharding import PartitionSpec as P


def shards(
    tokens, norm_gain, gate_weight, gate_scale, up_weight, up_scale, down_weight, down_scale
):
    flat = tokens.astype(jnp.float32)
    mean_square = jnp.mean(flat * flat, axis=-1, keepdims=True)
    inverse = lax.rsqrt(mean_square + 1e-06)
    normed = (flat * inverse * norm_gain).astype(jnp.bfloat16)
    group = lax.all_gather(normed, "tp", axis=0, tiled=True)
    gate_low = gate_weight.astype(jnp.bfloat16)
    up_low = up_weight.astype(jnp.bfloat16)
    down_low = down_weight.astype(jnp.bfloat16)
    gate = jnp.dot(
        group,
        lax.all_gather(gate_low, "fs", axis=0, tiled=True),
        preferred_element_type=jnp.float32,
    )
    up = jnp.dot(
        group, lax.all_gather(up_low, "fs", axis=0, tiled=True), preferred_element_type=jnp.float32
    )
    down_full = lax.all_gather(down_low, "fs", axis=1, tiled=True)
    gate = gate * gate_scale
    up = up * up_scale
    hidden = (jax.nn.silu(gate) * up).astype(jnp.bfloat16)
    scales = lax.all_gather(down_scale, "fs", axis=0, tiled=True)
    total = lax.psum_scatter(
        jnp.dot(hidden, down_full, preferred_element_type=jnp.float32).astype(jnp.bfloat16),
        "tp",
        scatter_dimension=0,
        tiled=True,
    ).astype(jnp.float32)
    return (total * scales).astype(jnp.bfloat16)


def solution(mesh):
    in_specs = (
        P(("rep", "fs", "tp"), None),
        P(),
        P("fs", "tp"),
        P("tp"),
        P("fs", "tp"),
        P("tp"),
        P("tp", "fs"),
        P("fs"),
    )
    out_specs = P(("rep", "fs", "tp"), None)
    return jax.shard_map(shards, mesh=mesh, in_specs=in_specs, out_specs=out_specs, check_vma=False)
```

profile of v0, /device:TPU:0, one launch (start us, length us, event | category | flops | bytes accessed | tf_op | source)
XLA Modules:
  0.0 408.0 jit_solution(18322760977833249545)
XLA Ops:
  6.5 1.2 fusion.2
  7.8 2.0 fusion.4
  9.8 0.0 all-gather.6.cloned.1.call-update
  9.8 0.0 all-gather.8.cloned.1.call-start
  9.9 3.3 convert_element_type.29
  13.2 0.0 all-gather.8.cloned.1.call-update
  13.2 0.0 all-gather.10.cloned.1.call-start
  13.2 1.3 convert_element_type.30
  14.5 0.0 all-gather.10.cloned.1.call-update
  14.5 0.0 copy-start.3
  14.6 0.0 all-gather.12.cloned.1.call-start
  14.6 3.1 convert_element_type.32
  17.8 0.0 all-gather.12.cloned.1.call-update
  17.8 0.0 reduce-scatter.2.cloned.1.call-start
  17.8 17.4 %all-gather.6.cloned.1.call-done = bf16[512,2048]{1,0:T(8,128)(2,1)} async-done(((bf16[128,2048]{1,0:T(8,128)(2,1)}), bf16[512,2048]{1,0:T(8,128)(2,1)}) %all-gather.6.cloned.1.call-update) | async-done | bytes 2097168 | tf_op jit(solution)/shard_map/all_gather | solution.py:14
  35.3 108.3 %all-gather.8.cloned.1.call-done = bf16[2048,1408]{1,0:T(8,128)(2,1)} async-done(((bf16[512,1408]{1,0:T(8,128)(2,1)}), bf16[2048,1408]{1,0:T(8,128)(2,1)}) %all-gather.8.cloned.1.call-update) | async-done | bytes 5767184 | tf_op jit(solution)/shard_map/all_gather | solution.py:20
  143.6 8.2 %convolution_multiply_fusion.1 = f32[512,1408]{1,0:T(8,128)} fusion(bf16[512,2048]{1,0:T(8,128)(2,1)} %all-gather.6.cloned.1.call-done, bf16[2048,1408]{1,0:T(8,128)(2,1)} %all-gather.8.cloned.1.call-done, f32[1408]{0:T(1024)S(1)} %copy-done.3), kind=kOutput, calls=%fused_computation.2 | convolution fusion | flops 2953510912 | bytes 10753536 | tf_op jit(solution)/shard_map/dot_general | solution.py:18
  151.8 98.3 %all-gather.10.cloned.1.call-done = bf16[2048,1408]{1,0:T(8,128)(2,1)} async-done(((bf16[512,1408]{1,0:T(8,128)(2,1)}), bf16[2048,1408]{1,0:T(8,128)(2,1)}) %all-gather.10.cloned.1.call-update) | async-done | bytes 5767184 | tf_op jit(solution)/shard_map/all_gather | solution.py:24
  250.1 106.4 %all-gather.12.cloned.1.call-done = bf16[1408,2048]{1,0:T(8,128)(2,1)} async-done(((bf16[1408,512]{1,0:T(8,128)(2,1)}), bf16[1408,2048]{1,0:T(8,128)(2,1)}) %all-gather.12.cloned.1.call-update) | async-done | bytes 5767184 | tf_op jit(solution)/shard_map/all_gather | solution.py:26
  356.5 13.4 %convolution_convert_fusion = bf16[512,2048]{1,0:T(8,128)(2,1)} fusion(bf16[1408,2048]{1,0:T(8,128)(2,1)} %all-gather.12.cloned.1.call-done, bf16[512,2048]{1,0:T(8,128)(2,1)S(1)} %copy-done.2, bf16[2048,1408]{1,0:T(8,128)(2,1)} %all-gather.10.cloned.1.call-done, f32[512,1408]{1,0:T(8,128)} %convolution_multiply_fusion.1, f32[1408]{0:T(1024)S(1)} %copy-done.4), kind=kOutput, calls=%fused_computation.4 | convolution fusion | flops 5911674880 | bytes 18617856 | tf_op jit(solution)/shard_map/dot_general | solution.py:32
  370.0 0.0 reduce-scatter.2.cloned.1.call-update
  370.0 11.9 %all-gather = f32[4,1,512]{2,1,0:T(1,128)S(1)} all-gather(f32[1,1,512]{2,1,0:T(1,128)S(1)} %bitcast.8), channel_id=1, replica_groups=mesh['rep'=2,'fs'=4,'tp'=4] {'fs'}, dimensions={0}, use_global_device_ids=true | all-gather | bytes 10240 | tf_op jit(solution)/shard_map/all_gather | solution.py:30
  381.9 17.6 %reduce-scatter.2.cloned.1.call-done = bf16[128,2048]{1,0:T(8,128)(2,1)} async-done(((bf16[512,2048]{1,0:T(8,128)(2,1)}), bf16[128,2048]{1,0:T(8,128)(2,1)}) %reduce-scatter.2.cloned.1.call-update) | async-done | bytes 524304 | tf_op jit(solution)/shard_map/reduce_scatter | solution.py:31
  399.6 1.9 multiply_convert_fusion
  (11 shorter events, 0.0 us)
Async XLA Ops:
  6.5 28.7 %all-gather.6.cloned.1.call-start = ((), (), s32[]{:S(2)}) async-start(), calls=%async_computation.1 | async-start | bytes 2621440 | tf_op jit(solution)/shard_map/all_gather | solution.py:14
  9.8 3.4 copy-start
  9.8 133.7 %all-gather.8.cloned.1.call-start = ((), (), s32[]{:S(2)}) async-start(), calls=%async_computation.2 | async-start | bytes 7208960 | tf_op jit(solution)/shard_map/all_gather | solution.py:20
  13.2 236.9 %all-gather.10.cloned.1.call-start = ((), (), s32[]{:S(2)}) async-start(), calls=%async_computation.3 | async-start | bytes 7208960 | tf_op jit(solution)/shard_map/all_gather | solution.py:24
  14.5 129.0 %copy-start.3 = (f32[1408]{0:T(1024)S(1)}, f32[1408]{0:T(1024)}, u32[]{:S(2)}) copy-start(f32[1408]{0:T(1024)} %param.11) | copy-start | bytes 16900
  14.6 342.0 %all-gather.12.cloned.1.call-start = ((), (), s32[]{:S(2)}) async-start(), calls=%async_computation.4 | async-start | bytes 7208960 | tf_op jit(solution)/shard_map/all_gather | solution.py:26
  17.8 338.7 %copy-start.4 = (f32[1408]{0:T(1024)S(1)}, f32[1408]{0:T(1024)}, u32[]{:S(2)}) copy-start(f32[1408]{0:T(1024)} %param.13) | copy-start | bytes 16900
  17.8 381.8 %reduce-scatter.2.cloned.1.call-start = ((), (), s32[]{:S(2)}) async-start(), calls=%async_computation.5 | async-start | bytes 2621440 | tf_op jit(solution)/shard_map/reduce_scatter | solution.py:31
  35.3 321.2 %copy-start.2 = (bf16[512,2048]{1,0:T(8,128)(2,1)S(1)}, bf16[512,2048]{1,0:T(8,128)(2,1)}, u32[]{:S(2)}) copy-start(bf16[512,2048]{1,0:T(8,128)(2,1)} %all-gather.6.cloned.1.call-done) | copy-start | bytes 6291460
  151.8 218.2 %copy-start.1 = (f32[512]{0:T(512)S(1)}, f32[512]{0:T(512)}, u32[]{:S(2)}) copy-start(f32[512]{0:T(512)} %param.15) | copy-start | bytes 6148
Sparse Core Ops, SparseCore 0:
  9.9 25.2 all-gather.5
  36.8 106.6 all-gather.7
  145.1 104.9 all-gather.9
  251.5 104.9 all-gather.11
  370.1 29.4 reduce-scatter.1
where the time goes:
time: 408 us
  waiting for transfers between devices  348 us (85%)
  matrix products  21.7 us (5%)
  between operations  13.2 us (3%)
  other arithmetic  12.9 us (3%)
  blocking collectives  11.9 us (3%)
    all_gather x1, waiting for transfers between devices, shards(): lax.all_gather(gate_low, 'fs', axis=0, tiled=True)  108 us
    all_gather x1, waiting for transfers between devices, shards(): down_full = lax.all_gather(down_low, 'fs', axis=1, tiled=True)  106 us
    all_gather x1, waiting for transfers between devices, shards(): lax.all_gather(up_low, 'fs', axis=0, tiled=True)  98.3 us
    reduce_scatter x1, waiting for transfers between devices, shards(): lax.psum_scatter(jnp.dot(hidden, down_full, preferred_element_type=jnp.fl...  17.6 us
    all_gather x1, waiting for transfers between devices, shards(): group = lax.all_gather(normed, 'tp', axis=0, tiled=True)  17.4 us
    dot_general x1, matrix products, shards(): jnp.dot(hidden, down_full, preferred_element_type=jnp.float32)  13.4 us
    all_gather x1, blocking collectives, shards(): scales = lax.all_gather(down_scale, 'fs', axis=0, tiled=True)  11.9 us
    dot_general x1, matrix products, shards(): jnp.dot(group, lax.all_gather(gate_low, 'fs', axis=0, tiled=True), prefer...  8.23 us
  transfers between devices with their start and end apart: 5, of which 5 were waited for; matrix products, arithmetic and copies ran while one was open for 4% of the time, Pallas kernels for 0%

commit v1 on v0

--- a/solution.py
+++ b/solution.py
@@ -23,7 +23,12 @@
     up = jnp.dot(
         group, lax.all_gather(up_low, "fs", axis=0, tiled=True), preferred_element_type=jnp.float32
     )
-    down_full = lax.all_gather(down_low, "fs", axis=1, tiled=True)
+    ring = [down_low]
+    for hop in range(3):
+        ring.append(lax.ppermute(ring[-1], "fs", [(dev, (dev + 1) % 4) for dev in range(4)]))
+    down_full = jnp.roll(
+        jnp.concatenate(ring[::-1], axis=1), (lax.axis_index("fs") + 1) * ring[0].shape[1], axis=1
+    )
     gate = gate * gate_scale
     up = up * up_scale
     hidden = (jax.nn.silu(gate) * up).astype(jnp.bfloat16)

time: 408 us -> 354 us (0.87)
  waiting for transfers between devices: 348 us -> 234 us
  starting transfers between devices: 0.17 us -> 43.7 us
  local copies, waits for them, and re-layouts: 0.03 us -> 14.2 us
    ppermute x0 -> x3, waiting for transfers between devices: none -> 147 us  [shards(): lax.ppermute(ring[-1], 'fs', [(dev, (dev + 1) % 4) for dev in range(4)])]
    all_gather x1, waiting for transfers between devices: 108 us -> 0.01 us  [shards(): lax.all_gather(gate_low, 'fs', axis=0, tiled=True)]
    all_gather x1 -> x0, waiting for transfers between devices: 106 us -> none  [shards(): down_full = lax.all_gather(down_low, 'fs', axis=1, tiled=True)]
    ppermute x0 -> x3, starting transfers between devices: none -> 43.6 us  [shards(): lax.ppermute(ring[-1], 'fs', [(dev, (dev + 1) % 4) for dev in range(4)])]
    all_gather x1, waiting for transfers between devices: 98.3 us -> 69.2 us  [shards(): lax.all_gather(up_low, 'fs', axis=0, tiled=True)]
    all_gather x1, waiting for transfers between devices: 17.4 us -> 0.01 us  [shards(): group = lax.all_gather(normed, 'tp', axis=0, tiled=True)]
    unnamed x10 -> x20, local copies, waits for them, and re-layouts: 0.03 us -> 14.2 us
  transfers between devices with their start and end apart: 5 -> 7, of which waited for: 5 -> 5; matrix products, arithmetic and copies ran while one was open for 4% -> 9% of each run, Pallas kernels for 0% -> 0%
where the time goes in v1:
time: 354 us
  waiting for transfers between devices  234 us (66%)
  starting transfers between devices  43.7 us (12%)
  matrix products  21.8 us (6%)
  other arithmetic  14.4 us (4%)
  local copies, waits for them, and re-layouts  14.2 us (4%)
  between operations  13.2 us (4%)
  blocking collectives  11.9 us (3%)
    ppermute x3, waiting for transfers between devices, shards(): lax.ppermute(ring[-1], 'fs', [(dev, (dev + 1) % 4) for dev in range(4)])  147 us
    all_gather x1, waiting for transfers between devices, shards(): lax.all_gather(up_low, 'fs', axis=0, tiled=True)  69.2 us
    ppermute x3, starting transfers between devices, shards(): lax.ppermute(ring[-1], 'fs', [(dev, (dev + 1) % 4) for dev in range(4)])  43.6 us
    reduce_scatter x1, waiting for transfers between devices, shards(): lax.psum_scatter(jnp.dot(hidden, down_full, preferred_element_type=jnp.fl...  18.2 us
    unnamed x20, local copies, waits for them, and re-layouts  14.2 us
    dot_general x1, matrix products, shards(): jnp.dot(hidden, down_full, preferred_element_type=jnp.float32)  13.3 us
    all_gather x1, blocking collectives, shards(): scales = lax.all_gather(down_scale, 'fs', axis=0, tiled=True)  11.9 us
    dot_general x1, matrix products, shards(): jnp.dot(group, lax.all_gather(gate_low, 'fs', axis=0, tiled=True), prefer...  8.5 us
  transfers between devices with their start and end apart: 7, of which 5 were waited for; matrix products, arithmetic and copies ran while one was open for 9% of the time, Pallas kernels for 0%

profile of v1, /device:TPU:0, one launch (start us, length us, event | category | flops | bytes accessed | tf_op | source)
XLA Modules:
  0.0 353.7 jit_solution(3308724839631174386)
XLA Ops:
  6.5 1.2 fusion.7
  7.8 2.0 fusion.9
  9.9 3.1 convert_element_type.29
  13.0 3.3 convert_element_type.30
  16.6 3.1 collective-permute-start
  19.7 37.7 %collective-permute-done = bf16[1408,512]{1,0:T(8,128)(2,1)S(1)} collective-permute-done((bf16[1408,512]{1,0:T(8,128)(2,1)S(1)}, bf16[1408,512]{1,0:T(8,128)(2,1)S(1)}, u32[]{:S(2)}, u32[]{:S(2)}) %collective-permute-start) | collective-permute-done | bytes 1441824 | tf_op jit(solution)/shard_map/ppermute | solution.py:28
  58.4 6.4 %collective-permute-start.1 = (bf16[1408,512]{1,0:T(8,128)(2,1)S(1)}, bf16[1408,512]{1,0:T(8,128)(2,1)}, u32[]{:S(2)}, u32[]{:S(2)}) collective-permute-start(bf16[1408,512]{1,0:T(8,128)(2,1)S(1)} %collective-permute-done), channel_id=1, source_target_pairs={{0,4},{4,8},{8,12},{12,0},{1,5},{5,9},{9,13},{13,1},{2,6},{6,10},{... | collective-permute-start | bytes 4325384 | tf_op jit(solution)/shard_map/ppermute | solution.py:28
  64.8 63.1 %collective-permute-done.1 = bf16[1408,512]{1,0:T(8,128)(2,1)} collective-permute-done((bf16[1408,512]{1,0:T(8,128)(2,1)S(1)}, bf16[1408,512]{1,0:T(8,128)(2,1)}, u32[]{:S(2)}, u32[]{:S(2)}) %collective-permute-start.1) | collective-permute-done | bytes 1441824 | tf_op jit(solution)/shard_map/ppermute | solution.py:28
  127.9 34.1 %collective-permute-start.2 = (bf16[1408,512]{1,0:T(8,128)(2,1)}, bf16[1408,512]{1,0:T(8,128)(2,1)}, u32[]{:S(2)}, u32[]{:S(2)}) collective-permute-start(bf16[1408,512]{1,0:T(8,128)(2,1)} %collective-permute-done.1), channel_id=1, source_target_pairs={{0,4},{4,8},{8,12},{12,0},{1,5},{5,9},{9,13},{13,1},{2,6},{6,10},{... | collective-permute-start | bytes 4325384 | tf_op jit(solution)/shard_map/ppermute | solution.py:28
  162.0 46.1 %collective-permute-done.2 = bf16[1408,512]{1,0:T(8,128)(2,1)} collective-permute-done((bf16[1408,512]{1,0:T(8,128)(2,1)}, bf16[1408,512]{1,0:T(8,128)(2,1)}, u32[]{:S(2)}, u32[]{:S(2)}) %collective-permute-start.2) | collective-permute-done | bytes 1441824 | tf_op jit(solution)/shard_map/ppermute | solution.py:28
  208.2 2.6 constant_dynamic-update-slice_fusion.7
  210.8 2.6 constant_dynamic-update-slice_fusion.6
  213.4 1.3 constant_dynamic-update-slice_fusion.5
  214.7 1.3 constant_dynamic-update-slice_fusion.4
  216.0 2.7 constant_dynamic-update-slice_fusion.3
  218.7 2.6 constant_dynamic-update-slice_fusion.2
  221.4 1.3 constant_dynamic-update-slice_fusion.1
  222.6 1.4 constant_dynamic-update-slice_fusion
  224.0 8.5 %convolution_multiply_fusion.1 = f32[512,1408]{1,0:T(8,128)} fusion(bf16[512,2048]{1,0:T(8,128)(2,1)} %all-gather.5.cloned.1.call-done, bf16[2048,1408]{1,0:T(8,128)(2,1)} %all-gather.7.cloned.1.call-done, f32[1408]{0:T(1024)S(1)} %copy-done.5), kind=kOutput, calls=%fused_computation.4 | convolution fusion | flops 2953510912 | bytes 10753536 | tf_op jit(solution)/shard_map/dot_general | solution.py:18
  232.5 69.2 %all-gather.9.cloned.1.call-done = bf16[2048,1408]{1,0:T(8,128)(2,1)} async-done(((bf16[512,1408]{1,0:T(8,128)(2,1)}), bf16[2048,1408]{1,0:T(8,128)(2,1)}) %all-gather.9.cloned.1.call-update) | async-done | bytes 5767184 | tf_op jit(solution)/shard_map/all_gather | solution.py:24
  301.7 13.3 %fusion.4 = bf16[512,2048]{1,0:T(8,128)(2,1)} fusion(bf16[1408,4096]{1,0:T(8,128)(2,1)} %constant_dynamic-update-slice_fusion, s32[]{:T(128)S(6)} %select_n.14, bf16[512,2048]{1,0:T(8,128)(2,1)S(1)} %copy-done.4, bf16[2048,1408]{1,0:T(8,128)(2,1)} %all-gather.9.cloned.1.call-done, f32[512,1408]{1,0:T(8,128)} %convolution_multiply_fusion.1, ...), kind=kOutput, calls=%fused_computation.6 | convolution fusion | flops 5911674880 | bytes 18617860 | tf_op jit(solution)/shard_map/dot_general | solution.py:37
  315.1 11.9 %all-gather = f32[4,1,512]{2,1,0:T(1,128)S(1)} all-gather(f32[1,1,512]{2,1,0:T(1,128)S(1)} %bitcast.7), channel_id=1, replica_groups=mesh['rep'=2,'fs'=4,'tp'=4] {'fs'}, dimensions={0}, use_global_device_ids=true | all-gather | bytes 10240 | tf_op jit(solution)/shard_map/all_gather | solution.py:35
  327.0 18.2 %reduce-scatter.2.cloned.1.call-done = bf16[128,2048]{1,0:T(8,128)(2,1)} async-done(((bf16[512,2048]{1,0:T(8,128)(2,1)}), bf16[128,2048]{1,0:T(8,128)(2,1)}) %reduce-scatter.2.cloned.1.call-update) | async-done | bytes 524304 | tf_op jit(solution)/shard_map/reduce_scatter | solution.py:36
  345.2 1.9 multiply_convert_fusion
  (26 shorter events, 1.5 us)
Async XLA Ops:
  6.5 217.5 %all-gather.5.cloned.1.call-start = ((), (), s32[]{:S(2)}) async-start(), calls=%async_computation.1 | async-start | bytes 2621440 | tf_op jit(solution)/shard_map/all_gather | solution.py:14
  9.8 214.2 %all-gather.7.cloned.1.call-start = ((), (), s32[]{:S(2)}) async-start(), calls=%async_computation.2 | async-start | bytes 7208960 | tf_op jit(solution)/shard_map/all_gather | solution.py:20
  13.0 3.4 copy-start
  13.0 288.8 %all-gather.9.cloned.1.call-start = ((), (), s32[]{:S(2)}) async-start(), calls=%async_computation.3 | async-start | bytes 7208960 | tf_op jit(solution)/shard_map/all_gather | solution.py:24
  16.3 328.9 %reduce-scatter.2.cloned.1.call-start = ((), (), s32[]{:S(2)}) async-start(), calls=%async_computation.4 | async-start | bytes 2621440 | tf_op jit(solution)/shard_map/reduce_scatter | solution.py:36
  16.6 40.8 %collective-permute-start = (bf16[1408,512]{1,0:T(8,128)(2,1)S(1)}, bf16[1408,512]{1,0:T(8,128)(2,1)S(1)}, u32[]{:S(2)}, u32[]{:S(2)}) collective-permute-start(bf16[1408,512]{1,0:T(8,128)(2,1)S(1)} %convert_element_type.32), channel_id=1, source_target_pairs={{0,4},{4,8},{8,12},{12,0},{1,5},{5,9},{9,13},{13,1},{2,6},{6,10},{... | collective-permute-start | bytes 4325384 | tf_op jit(solution)/shard_map/ppermute | solution.py:28
  57.3 1.1 copy-start.1
  58.4 69.5 %collective-permute-start.1 = (bf16[1408,512]{1,0:T(8,128)(2,1)S(1)}, bf16[1408,512]{1,0:T(8,128)(2,1)}, u32[]{:S(2)}, u32[]{:S(2)}) collective-permute-start(bf16[1408,512]{1,0:T(8,128)(2,1)S(1)} %collective-permute-done), channel_id=1, source_target_pairs={{0,4},{4,8},{8,12},{12,0},{1,5},{5,9},{9,13},{13,1},{2,6},{6,10},{... | collective-permute-start | bytes 4325384 | tf_op jit(solution)/shard_map/ppermute | solution.py:28
  127.9 80.2 %collective-permute-start.2 = (bf16[1408,512]{1,0:T(8,128)(2,1)}, bf16[1408,512]{1,0:T(8,128)(2,1)}, u32[]{:S(2)}, u32[]{:S(2)}) collective-permute-start(bf16[1408,512]{1,0:T(8,128)(2,1)} %collective-permute-done.1), channel_id=1, source_target_pairs={{0,4},{4,8},{8,12},{12,0},{1,5},{5,9},{9,13},{13,1},{2,6},{6,10},{... | collective-permute-start | bytes 4325384 | tf_op jit(solution)/shard_map/ppermute | solution.py:28
  162.0 51.4 %copy-start.2 = (bf16[1408,512]{1,0:T(8,128)(2,1)S(1)}, bf16[1408,512]{1,0:T(8,128)(2,1)}, u32[]{:S(2)}) copy-start(bf16[1408,512]{1,0:T(8,128)(2,1)} %copy-done.1) | copy-start | bytes 4325380
  222.6 1.4 copy-start.5
  224.0 77.7 %copy-start.6 = (f32[1408]{0:T(1024)S(1)}, f32[1408]{0:T(1024)}, u32[]{:S(2)}) copy-start(f32[1408]{0:T(1024)} %param.13) | copy-start | bytes 16900
  224.0 77.7 %copy-start.4 = (bf16[512,2048]{1,0:T(8,128)(2,1)S(1)}, bf16[512,2048]{1,0:T(8,128)(2,1)}, u32[]{:S(2)}) copy-start(bf16[512,2048]{1,0:T(8,128)(2,1)} %all-gather.5.cloned.1.call-done) | copy-start | bytes 6291460
  232.5 82.6 %copy-start.3 = (f32[512]{0:T(512)S(1)}, f32[512]{0:T(512)}, u32[]{:S(2)}) copy-start(f32[512]{0:T(512)} %param.15) | copy-start | bytes 6148
Sparse Core Ops, SparseCore 0:
  9.9 25.2 all-gather.4
  36.8 157.6 all-gather.6
  196.2 105.5 all-gather.8
  315.2 29.9 reduce-scatter.1
